TPU v7x, 32 devices: a whole 2x2x4 slice. The times are simulated.
32 devices in a mesh: ep: 8 (over z, core), tp: 4 (over y, x).
Axes of the slice: x: 2, y: 2, z: 4, core: 2. Of those that a mesh axis runs over, the one named last changes fastest.
Arguments:
- mix_in: bfloat16 [2048, 2048], P('ep'), may hold values from -6 to 6
- mix_gain: float32 [2048], replicated, may hold values from 0.1 to 1.9
- w_in_x: bfloat16 [2048, 2048], P(None, 'tp'), may hold values from -0.125 to 0.125
- w_in_y: bfloat16 [2048, 2048], P(None, 'tp'), may hold values from -0.125 to 0.125
- conv_taps: float32 [4, 2048], P(None, 'tp'), may hold values from -3 to 3
- recur_gate_w: bfloat16 [16, 128, 128], P('tp'), may hold values from -0.5 to 0.5
- input_gate_w: bfloat16 [16, 128, 128], P('tp'), may hold values from -0.5 to 0.5
- decay_logit: float32 [2048], P('tp'), may hold values from 4 to 20
- decay_shift: float32 [2048, 2048], P('ep', 'tp'), may hold values from -2.2 to 0
- moe_in: bfloat16 [2048, 2048], P('ep'), may hold values from -6 to 6
- moe_gain: float32 [2048], replicated, may hold values from 0.1 to 1.9
- routes: int32 [2048, 2], P('ep'), may hold values from 0 to 7, all different within a row; in each aligned block of 256 rows (0 to 255, 256 to 511, ...) at most 128 rows name the same one
- route_weight: float32 [2048, 2], P('ep'), may hold values from 0.1 to 1
- expert_gate: bfloat16 [8, 2048, 2048], P('ep', None, 'tp'), may hold values from -0.125 to 0.125
- expert_up: bfloat16 [8, 2048, 2048], P('ep', None, 'tp'), may hold values from -0.125 to 0.125
- expert_down: bfloat16 [8, 2048, 2048], P('ep', None, 'tp'), may hold values from -0.125 to 0.125
Outputs:
- mixer_out: bfloat16 [2048, 2048], P('ep', 'tp')
- moe_out: bfloat16 [2048, 2048], P('ep', 'tp')
Inputs may be any that keep to these rules, and one draw needn't show every extreme that they name: `routes`: each row names 2 different experts. Among the rows of one index of ep no expert is named more than 128 times, a bound that some block reaches.
All inputs are finite; a program needn't handle non-finite values.
Results may differ from a plain program's by a relative error of at most 0.0095.
Values may be sent and summed in bfloat16 or wider, within the bound.
A program may use at most 64 MiB of HBM per device.

v0:
```python
import jax
import jax.numpy as jnp
from jax import lax
from jax.sharding import PartitionSpec as P

epsilon = 1e-06
lru_scale = 8.0


def from_behind(value, axis, by):
    count = lax.axis_size(axis)
    pairs = [(i, i + by) for i in range(count) if 0 <= i + by < count]
    return lax.ppermute(value, axis, pairs)


def entering(value, axis, combine, identity):
    count, index = (lax.axis_size(axis), lax.axis_index(axis))
    everything = jax.tree.map(lambda part: lax.all_gather(part, axis), value)
    start = jax.tree.map(
        lambda part, zero: jnp.broadcast_to(jnp.asarray(zero, part.dtype), part.shape),
        value,
        identity,
    )

    def hop(k, before):
        reached = k < index
        new = combine(before, jax.tree.map(lambda part: part[k], everything))
        return jax.tree.map(lambda a, b: jnp.where(reached, a, b), new, before)

    return lax.fori_loop(0, count, hop, start)


def norm_rows(rows, gain):
    widened = rows.astype(jnp.float32)
    scaled = widened * lax.rsqrt(jnp.mean(widened * widened, axis=-1, keepdims=True) + epsilon)
    return (scaled * gain[None, :]).astype(jnp.bfloat16)


def link(earlier, later):
    return (earlier[0] * later[0], later[0] * earlier[1] + later[1])


def local(
    mix_in,
    mix_gain,
    w_in_x,
    w_in_y,
    conv_taps,
    recur_gate_w,
    input_gate_w,
    decay_logit,
    decay_shift,
    moe_in,
    moe_gain,
    routes,
    route_weight,
    expert_gate,
    expert_up,
    expert_down,
):
    row_count = mix_in.shape[0]
    width_dev = w_in_x.shape[1]
    heads_dev = recur_gate_w.shape[0]
    block_size = recur_gate_w.shape[1]
    tap_count = conv_taps.shape[0]
    mixer_rows = norm_rows(mix_in, mix_gain)
    x_branch = jnp.dot(mixer_rows, w_in_x, preferred_element_type=jnp.float32).astype(jnp.bfloat16)
    y_branch = jnp.dot(mixer_rows, w_in_y, preferred_element_type=jnp.float32).astype(jnp.bfloat16)
    previous = from_behind(x_branch[row_count - (tap_count - 1) :], "ep", 1)
    padded = jnp.concatenate([previous, x_branch], axis=0)
    conv_sum = jnp.zeros((row_count, width_dev), jnp.float32)
    for tap_index in range(tap_count):
        conv_sum = conv_sum + conv_taps[tap_index][None, :] * padded[
            tap_index : tap_index + row_count
        ].astype(jnp.float32)
    x_conv = conv_sum.astype(jnp.bfloat16)
    heads_in = x_conv.reshape(row_count, heads_dev, block_size)
    gate_a = jnp.einsum(
        "thi,hij->thj", heads_in, recur_gate_w, preferred_element_type=jnp.float32
    ).reshape(row_count, width_dev)
    gate_x = jnp.einsum(
        "thi,hij->thj", heads_in, input_gate_w, preferred_element_type=jnp.float32
    ).reshape(row_count, width_dev)
    log_decay = (
        -lru_scale * jax.nn.sigmoid(gate_a) * jax.nn.softplus(-decay_logit)[None, :] + decay_shift
    )
    lru_drive = (
        jnp.sqrt(-jnp.expm1(2.0 * log_decay)) * jax.nn.sigmoid(gate_x) * x_conv.astype(jnp.float32)
    )
    through, local_state = lax.associative_scan(link, (jnp.exp(log_decay), lru_drive), axis=0)
    identity = (jnp.ones((width_dev,), jnp.float32), jnp.zeros((width_dev,), jnp.float32))
    carried = entering((through[row_count - 1], local_state[row_count - 1]), "ep", link, identity)
    lru_state = local_state + through * carried[1][None, :]
    mixer_out = (lru_state * jax.nn.gelu(y_branch.astype(jnp.float32))).astype(jnp.bfloat16)
    moe_rows = norm_rows(moe_in, moe_gain)
    token_count = moe_rows.shape[0]
    feature_count = moe_rows.shape[1]
    choose_count = routes.shape[1]
    expert_count = lax.axis_size("ep")
    capacity = 2 * token_count * choose_count // expert_count
    slot_total = expert_count * capacity
    expert_ids = routes.reshape(-1)
    onehot = (expert_ids[:, None] == jnp.arange(expert_count, dtype=jnp.int32)[None, :]).astype(
        jnp.int32
    )
    slot_rank = jnp.sum(jnp.cumsum(onehot, axis=0) * onehot, axis=1) - 1
    slot_index = expert_ids * capacity + slot_rank
    token_index = jnp.repeat(jnp.arange(token_count, dtype=jnp.int32), choose_count)
    slot_owner = jnp.full((slot_total,), token_count, jnp.int32).at[slot_index].set(token_index)
    padded_rows = jnp.concatenate([moe_rows, jnp.zeros((1, feature_count), jnp.bfloat16)], axis=0)
    outgoing = padded_rows[slot_owner].reshape(expert_count, capacity, feature_count)
    column_width = feature_count // lax.axis_size("tp")
    own_columns = lax.dynamic_slice_in_dim(
        outgoing, lax.axis_index("tp") * column_width, column_width, 2
    )
    incoming = lax.all_to_all(own_columns, "ep", split_axis=0, concat_axis=0, tiled=True)
    piece = lax.all_gather(incoming, "tp", axis=2, tiled=True)
    flat_rows = piece.reshape(slot_total, piece.shape[2])
    gate_rows = expert_gate[0]
    up_rows = expert_up[0]
    gate_proj = jnp.dot(flat_rows, gate_rows, preferred_element_type=jnp.float32)
    up_proj = jnp.dot(flat_rows, up_rows, preferred_element_type=jnp.float32)
    hidden = (jax.nn.silu(gate_proj) * up_proj).astype(jnp.bfloat16)
    down_rows = expert_down[0]
    columns = jnp.dot(
        lax.all_gather(hidden, "tp", axis=1, tiled=True),
        down_rows,
        preferred_element_type=jnp.float32,
    )
    results = columns.astype(jnp.bfloat16).reshape(expert_count, capacity, expert_down.shape[2])
    returned = lax.all_to_all(results, "ep", split_axis=0, concat_axis=0, tiled=True).reshape(
        slot_total, expert_down.shape[2]
    )
    picked = (
        returned[slot_index]
        .astype(jnp.float32)
        .reshape(token_count, choose_count, expert_down.shape[2])
    )
    route_share = route_weight / jnp.sum(route_weight, axis=1, keepdims=True)
    moe_out = jnp.sum(route_share[:, :, None] * picked, axis=1).astype(jnp.bfloat16)
    return (mixer_out, moe_out)


def solution(mesh):
    placed = (
        P("ep", None),
        P(),
        P(None, "tp"),
        P(None, "tp"),
        P(None, "tp"),
        P("tp", None, None),
        P("tp", None, None),
        P("tp"),
        P("ep", "tp"),
        P("ep", None),
        P(),
        P("ep", None),
        P("ep", None),
        P("ep", None, "tp"),
        P("ep", None, "tp"),
        P("ep", None, "tp"),
    )
    return jax.shard_map(
        local, mesh=mesh, in_specs=placed, out_specs=(P("ep", "tp"), P("ep", "tp")), check_vma=False
    )
```

profile of v0, /device:TPU:0, one launch (start us, length us, event | category | flops | bytes accessed | tf_op | source)
XLA Modules:
  0.0 283.7 jit_solution(14209495019624665678)
XLA Ops:
  11.2 2.4 scatter_custom_fusion
  15.6 6.0 %gather_fusion = bf16[1024,2048]{1,0:T(8,128)(2,1)} fusion(bf16[257,2048]{1,0:T(8,128)(2,1)S(1)} %concatenate.63, s32[1024]{0:T(1024)S(1)} %fusion.50), kind=kCustom, calls=%fused_computation | custom fusion | bytes 8392704 | tf_op jit(solution)/shard_map/gather | solution.py:111
  22.9 33.0 %all_to_all.10 = bf16[8,128,512]{2,1,0:T(8,128)(2,1)} all-to-all(bf16[8,128,512]{2,1,0:T(8,128)(2,1)S(1)} %constant_dynamic-slice_fusion.2), channel_id=1, replica_groups=mesh['ep'=8,'tp'=4] {'ep'}, dimensions={0} | all-to-all | bytes 2097152 | tf_op jit(solution)/shard_map/all_to_all | solution.py:116
  56.8 2.4 convolution_convert_fusion.1
  59.9 1.5 collective-permute-start
  63.0 1.7 add_convert_fusion
  64.7 42.8 %all-gather.5.cloned.1.call-done = bf16[8,128,2048]{2,1,0:T(8,128)(2,1)} async-done(((bf16[8,128,512]{2,1,0:T(8,128)(2,1)}), bf16[8,128,2048]{2,1,0:T(8,128)(2,1)}) %all-gather.5.cloned.1.call-update) | async-done | bytes 4194320 | tf_op jit(solution)/shard_map/all_gather | solution.py:117
  107.4 4.7 %fusion.8 = f32[1024,512]{1,0:T(8,128)S(1)} fusion(bf16[1024,2048]{1,0:T(8,128)(2,1)} %bitcast.86, bf16[1,2048,512]{2,1,0:T(8,128)(2,1)S(1)} %copy-done), kind=kOutput, calls=%fused_computation.18 | convolution fusion | flops 2147483648 | bytes 8388608 | tf_op jit(solution)/shard_map/dot_general | solution.py:122
  112.1 3.7 %multiply_convert_fusion = bf16[1024,512]{1,0:T(8,128)(2,1)} fusion(f32[1024,512]{1,0:T(8,128)S(1)} %fusion.8, bf16[1024,2048]{1,0:T(8,128)(2,1)S(1)} %bitcast.87, bf16[1,2048,512]{2,1,0:T(8,128)(2,1)S(1)} %copy-done.24), kind=kOutput, calls=%fused_computation.22 | convolution fusion | flops 2150629376 | bytes 9437184 | tf_op jit(solution)/shard_map/dot_general | solution.py:121
  118.5 1.8 convert_multiply_fusion.4
  125.8 2.0 multiply_add_fusion.1
  127.8 1.6 slice.283
  129.4 1.6 slice.284
  132.4 1.8 multiply_add_fusion.2
  135.5 1.5 slice.288
  137.0 1.5 slice.292
  138.6 1.6 multiply_add_fusion.3
  178.7 1.5 slice.287
  182.9 1.6 slice.330
  199.8 1.7 pad.114
  201.7 1.9 fusion.39
  204.4 12.8 %all-gather.1 = f32[8,1,512]{2,1,0:T(1,128)S(1)} all-gather(f32[1,1,512]{2,1,0:T(1,128)S(1)} %add_bitcast_fusion), channel_id=1, replica_groups=mesh['ep'=8,'tp'=4] {'ep'}, dimensions={0}, use_global_device_ids=true | all-gather | bytes 18432 | tf_op jit(solution)/shard_map/all_gather | solution.py:18
  217.2 1.7 pad.130
  218.9 1.6 pad.129
  221.3 12.8 %all-gather = f32[8,1,512]{2,1,0:T(1,128)S(1)} all-gather(f32[1,1,512]{2,1,0:T(1,128)S(1)} %add_bitcast_fusion.1), channel_id=1, replica_groups=mesh['ep'=8,'tp'=4] {'ep'}, dimensions={0}, use_global_device_ids=true | all-gather | bytes 18432 | tf_op jit(solution)/shard_map/all_gather | solution.py:18
  234.1 6.2 %fusion.14 = bf16[1024,512]{1,0:T(8,128)(2,1)} fusion(bf16[1024,2048]{1,0:T(8,128)(2,1)} %all-gather.7.cloned.1.call-done, bf16[1,2048,512]{2,1,0:T(8,128)(2,1)} %param.33), kind=kOutput, calls=%fused_computation.23 | convolution fusion | flops 2148007936 | bytes 7340032 | tf_op jit(solution)/shard_map/dot_general | solution.py:125
  240.3 3.9 %all-to-all-start.1 = ((bf16[8,128,512]{2,1,0:T(8,128)(2,1)}), bf16[8,128,512]{2,1,0:T(8,128)(2,1)S(1)}, u32[]{:S(2)}, u32[]{:S(2)}) async-start(bf16[8,128,512]{2,1,0:T(8,128)(2,1)} %bitcast.72), calls=%async_computation.1 | async-start | bytes 2097152 | tf_op jit(solution)/shard_map/all_to_all | solution.py:131
  244.7 4.1 %fusion.32 = bf16[256,512]{1,0:T(8,128)(2,1)} fusion(bf16[2048,512]{1,0:T(8,128)(2,1)} %param.21, f32[256,512]{1,0:T(8,128)} %pad.129, f32[256,512]{1,0:T(8,128)} %pad.130, f32[256,512]{1,0:T(8,128)} %copy-done.4, f32[256,512]{1,0:T(8,128)} %pad.114, bf16[256,2048]{1,0:T(8,128)(2,1)} %param.18, f32[2048]{0:T(1024)S(1)} %copy-done.28, ...), kind=kOutput, calls=%fused_computation.45 | convolution fusion | flops 541065216 | bytes 5516288 | tf_op jit(solution)/shard_map/dot_general | solution.py:68
  248.8 21.7 %all-to-all-done.1 = bf16[8,128,512]{2,1,0:T(8,128)(2,1)S(1)} async-done(((bf16[8,128,512]{2,1,0:T(8,128)(2,1)}), bf16[8,128,512]{2,1,0:T(8,128)(2,1)S(1)}, u32[]{:S(2)}, u32[]{:S(2)}) %all-to-all-start.1) | async-done | bytes 1048608 | tf_op jit(solution)/shard_map/all_to_all | solution.py:131
  270.5 2.6 gather_fusion.1
  273.1 1.7 reshape.120
  274.8 2.1 multiply_reduce_fusion
  (229 shorter events, 79.7 us)
Async XLA Ops:
  7.2 100.3 %copy-start = (bf16[1,2048,512]{2,1,0:T(8,128)(2,1)S(1)}, bf16[1,2048,512]{2,1,0:T(8,128)(2,1)}, u32[]{:S(2)}) copy-start(bf16[1,2048,512]{2,1,0:T(8,128)(2,1)} %param.32) | copy-start | bytes 6291460
  7.2 8.0 %copy-start.1 = (bf16[256,2048]{1,0:T(8,128)(2,1)S(1)}, bf16[256,2048]{1,0:T(8,128)(2,1)}, u32[]{:S(2)}) copy-start(bf16[256,2048]{1,0:T(8,128)(2,1)} %param.27) | copy-start | bytes 3145732
  7.2 8.0 %copy-start.12 = (f32[2048]{0:T(1024)S(1)}, f32[2048]{0:T(1024)}, u32[]{:S(2)}) copy-start(f32[2048]{0:T(1024)} %param.28) | copy-start | bytes 24580
  7.2 100.2 %all-gather.5.cloned.1.call-start = ((), (), s32[]{:S(2)}) async-start(), calls=%async_computation.2 | async-start | bytes 5242880 | tf_op jit(solution)/shard_map/all_gather | solution.py:117
  22.9 33.1 %copy-start.2 = (bf16[256,2048]{1,0:T(8,128)(2,1)S(1)}, bf16[256,2048]{1,0:T(8,128)(2,1)}, u32[]{:S(2)}) copy-start(bf16[256,2048]{1,0:T(8,128)(2,1)} %param.18) | copy-start | bytes 3145732
  22.9 33.9 %copy-start.27 = (f32[2048]{0:T(1024)S(1)}, f32[2048]{0:T(1024)}, u32[]{:S(2)}) copy-start(f32[2048]{0:T(1024)} %param.19) | copy-start | bytes 24580
  55.9 178.2 %all-gather.7.cloned.1.call-start = ((), (), s32[]{:S(2)}) async-start(), calls=%async_computation.3 | async-start | bytes 5242880 | tf_op jit(solution)/shard_map/all_gather | solution.py:126
  56.8 4.7 %copy-start.18 = (f32[256,2]{0,1:T(2,128)S(1)}, f32[256,2]{0,1:T(2,128)}, u32[]{:S(2)}) copy-start(f32[256,2]{0,1:T(2,128)} %param.30) | copy-start | bytes 6148
  56.8 4.7 %copy-start.20 = (f32[512]{0:T(512)S(1)}, f32[512]{0:T(512)}, u32[]{:S(2)}) copy-start(f32[512]{0:T(512)} %param.25) | copy-start | bytes 6148
  56.8 4.7 %copy-start.19 = (f32[4,512]{1,0:T(4,128)S(1)}, f32[4,512]{1,0:T(4,128)}, u32[]{:S(2)}) copy-start(f32[4,512]{1,0:T(4,128)} %param.22) | copy-start | bytes 24580
  59.2 0.7 copy-start.7
  59.9 3.0 %collective-permute-start = (bf16[3,512]{1,0:T(4,128)(2,1)S(1)}, bf16[3,512]{1,0:T(4,128)(2,1)S(1)}, u32[]{:S(2)}, u32[]{:S(2)}) collective-permute-start(bf16[3,512]{1,0:T(4,128)(2,1)S(1)} %slice.356), channel_id=1, source_target_pairs={{0,4},{4,8},{8,12},{12,16},{16,20},{20,24},{24,28},{1,5},{5,9},{9,... | collective-permute-start | bytes 9224 | tf_op jit(solution)/shard_map/ppermute | solution.py:13
  107.4 4.7 %copy-start.23 = (bf16[8,128,2048]{2,1,0:T(8,128)(2,1)S(1)}, bf16[8,128,2048]{2,1,0:T(8,128)(2,1)}, u32[]{:S(2)}) copy-start(bf16[8,128,2048]{2,1,0:T(8,128)(2,1)} %all-gather.5.cloned.1.call-done) | copy-start | bytes 12582916
  107.4 4.7 %copy-start.24 = (bf16[1,2048,512]{2,1,0:T(8,128)(2,1)S(1)}, bf16[1,2048,512]{2,1,0:T(8,128)(2,1)}, u32[]{:S(2)}) copy-start(bf16[1,2048,512]{2,1,0:T(8,128)(2,1)} %param.31) | copy-start | bytes 6291460
  112.1 3.7 %copy-start.25 = (bf16[4,128,128]{2,1,0:T(8,128)(2,1)S(1)}, bf16[4,128,128]{2,1,0:T(8,128)(2,1)}, u32[]{:S(2)}) copy-start(bf16[4,128,128]{2,1,0:T(8,128)(2,1)} %param.23) | copy-start | bytes 393220
  115.8 1.4 copy-start.26
  186.4 12.3 %copy-start.8 = (f32[31,512]{1,0:T(8,128)S(1)}, f32[31,512]{1,0:T(8,128)}, u32[]{:S(2)}) copy-start(f32[31,512]{1,0:T(8,128)} %slice.287) | copy-start | bytes 190468
  186.4 12.3 %copy-start.9 = (f32[31,512]{1,0:T(8,128)S(1)}, f32[31,512]{1,0:T(8,128)}, u32[]{:S(2)}) copy-start(f32[31,512]{1,0:T(8,128)} %slice.328) | copy-start | bytes 190468
  189.8 9.0 %copy-start.17 = (f32[1,512]{1,0:T(1,128)S(1)}, f32[1,512]{1,0:T(1,128)}, u32[]{:S(2)}) copy-start(f32[1,512]{1,0:T(1,128)} %slice.389) | copy-start | bytes 6148
  194.2 5.4 %copy-start.6 = (f32[63,512]{1,0:T(8,128)S(1)}, f32[63,512]{1,0:T(8,128)}, u32[]{:S(2)}) copy-start(f32[63,512]{1,0:T(8,128)} %slice.330) | copy-start | bytes 387076
  197.9 1.8 copy-start.16
  199.5 2.0 copy-start.15
  201.5 2.1 copy-start.14
  201.7 17.2 %copy-start.13 = (f32[1,512]{1,0:T(1,128)S(1)}, f32[1,512]{1,0:T(1,128)}, u32[]{:S(2)}) copy-start(f32[1,512]{1,0:T(1,128)} %slice.387) | copy-start | bytes 6148
  203.6 15.3 %copy-start.3 = (f32[127,512]{1,0:T(8,128)S(1)}, f32[127,512]{1,0:T(8,128)}, u32[]{:S(2)}) copy-start(f32[127,512]{1,0:T(8,128)} %get-tuple-element.130) | copy-start | bytes 780292
  203.7 36.6 %copy-start.4 = (f32[256,512]{1,0:T(8,128)}, f32[256,512]{1,0:T(8,128)S(1)}, u32[]{:S(2)}) copy-start(f32[256,512]{1,0:T(8,128)S(1)} %pad.113) | copy-start | bytes 1572868
  240.3 3.9 %copy-start.10 = (f32[512]{0:T(512)S(1)}, f32[512]{0:T(512)}, u32[]{:S(2)}) copy-start(f32[512]{0:T(512)} %custom-call) | copy-start | bytes 6148
  240.3 4.4 %copy-start.22 = (f32[256]{0:T(256)S(1)}, f32[256]{0:T(256)}, u32[]{:S(2)}) copy-start(f32[256]{0:T(256)} %copy-done.21) | copy-start | bytes 3076
  240.3 4.4 %copy-start.28 = (f32[2048]{0:T(1024)S(1)}, f32[2048]{0:T(1024)}, u32[]{:S(2)}) copy-start(f32[2048]{0:T(1024)} %param.19) | copy-start | bytes 24580
  240.3 30.2 %all-to-all-start.1 = ((bf16[8,128,512]{2,1,0:T(8,128)(2,1)}), bf16[8,128,512]{2,1,0:T(8,128)(2,1)S(1)}, u32[]{:S(2)}, u32[]{:S(2)}) async-start(bf16[8,128,512]{2,1,0:T(8,128)(2,1)} %bitcast.72), calls=%async_computation.1 | async-start | bytes 2097152 | tf_op jit(solution)/shard_map/all_to_all | solution.py:131
  244.7 25.8 %copy-start.11 = (s32[1024]{0:T(1024)S(1)}, s32[1024]{0:T(1024)}, u32[]{:S(2)}) copy-start(s32[1024]{0:T(1024)} %pad_clamp_fusion) | copy-start | bytes 12292
  270.5 4.3 %copy-start.5 = (f32[256,2]{1,0:T(8,128)S(1)}, f32[256,2]{1,0:T(8,128)}, u32[]{:S(2)}) copy-start(f32[256,2]{1,0:T(8,128)} %copy.41) | copy-start | bytes 6148
  (1 other events, 0.6 us)
Sparse Core Ops, SparseCore 0:
  56.0 51.3 all-gather.4
  115.9 52.4 all-gather.6
where the time goes:
time: 286 us; the launch traced here: 284 us
  local copies, waits for them, and re-layouts  86.2 us (30%)
  waiting for transfers between devices  64.5 us (23%)
  blocking collectives  58.5 us (20%)
  other arithmetic  32.3 us (11%)
  matrix products  21.7 us (8%)
  between operations  14.8 us (5%)
  starting transfers between devices  5.54 us (2%)
    slice x52, local copies, waits for them, and re-layouts, local(): lax.associative_scan(link, (jnp.exp(log_decay), lru_drive), axis=0)  60.4 us
    all_gather x1, waiting for transfers between devices, local(): piece = lax.all_gather(incoming, 'tp', axis=2, tiled=True)  42.8 us
    all_to_all x1, blocking collectives, local(): lax.all_to_all(own_columns, 'ep', split_axis=0, concat_axis=0, tiled=True)  33 us
    all_gather x2, blocking collectives, entering(): everything = jax.tree.map(lambda part: lax.all_gather(part, axis), value)  25.6 us
    all_to_all x1, waiting for transfers between devices, local(): lax.all_to_all(results, 'ep', split_axis=0, concat_axis=0, tiled=True)  21.7 us
    add x13, other arithmetic, link(): return (earlier[0] * later[0], later[0] * earlier[1] + later[1])  14.6 us
    dot_general x1, matrix products, local(): jnp.dot(lax.all_gather(hidden, 'tp', axis=1, tiled=True), down_rows, pref...  6.22 us
    gather x1, local copies, waits for them, and re-layouts, local(): padded_rows[slot_owner].reshape(expert_count, capacity, feature_count)  5.98 us
  transfers between devices with their start and end apart: 4, of which 2 were waited for; matrix products, arithmetic and copies ran while one was open for 36% of the time, Pallas kernels for 0%

commit v1 on v0

--- a/solution.py
+++ b/solution.py
@@ -114,7 +114,12 @@
         outgoing, lax.axis_index("tp") * column_width, column_width, 2
     )
     incoming = lax.all_to_all(own_columns, "ep", split_axis=0, concat_axis=0, tiled=True)
-    piece = lax.all_gather(incoming, "tp", axis=2, tiled=True)
+    ring = [incoming]
+    for hop_ in range(3):
+        ring.append(lax.ppermute(ring[-1], "tp", [(dev, (dev + 1) % 4) for dev in range(4)]))
+    piece = jnp.roll(
+        jnp.concatenate(ring[::-1], axis=2), (lax.axis_index("tp") + 1) * ring[0].shape[2], axis=2
+    )
     flat_rows = piece.reshape(slot_total, piece.shape[2])
     gate_rows = expert_gate[0]
     up_rows = expert_up[0]

time: 286 us -> 314 us (1.098)
  waiting for transfers between devices: 64.5 us -> 87.2 us
  local copies, waits for them, and re-layouts: 86.2 us -> 93.1 us
  matrix products: 21.7 us -> 17.7 us
    ppermute x0 -> x3, waiting for transfers between devices: none -> 65.5 us  [local(): lax.ppermute(ring[-1], 'tp', [(dev, (dev + 1) % 4) for dev in range(4)])]
    all_gather x1 -> x0, waiting for transfers between devices: 42.8 us -> none  [local(): piece = lax.all_gather(incoming, 'tp', axis=2, tiled=True)]
    unnamed x61 -> x72, local copies, waits for them, and re-layouts: 2.35 us -> 8.73 us
  transfers between devices with their start and end apart: 4 -> 6, of which waited for: 2 -> 4; matrix products, arithmetic and copies ran while one was open for 36% -> 32% of each run, Pallas kernels for 0% -> 0%
where the time goes in v1:
time: 314 us; the launch traced here: 311 us
  local copies, waits for them, and re-layouts  93.1 us (30%)
  waiting for transfers between devices  87.2 us (28%)
  blocking collectives  58.4 us (19%)
  other arithmetic  32.3 us (10%)
  matrix products  17.7 us (6%)
  between operations  14.9 us (5%)
  starting transfers between devices  7.5 us (2%)
    ppermute x3, waiting for transfers between devices, local(): lax.ppermute(ring[-1], 'tp', [(dev, (dev + 1) % 4) for dev in range(4)])  65.5 us
    slice x52, local copies, waits for them, and re-layouts, local(): lax.associative_scan(link, (jnp.exp(log_decay), lru_drive), axis=0)  60.4 us
    all_to_all x1, blocking collectives, local(): lax.all_to_all(own_columns, 'ep', split_axis=0, concat_axis=0, tiled=True)  32.8 us
    all_gather x2, blocking collectives, entering(): everything = jax.tree.map(lambda part: lax.all_gather(part, axis), value)  25.5 us
    all_to_all x1, waiting for transfers between devices, local(): lax.all_to_all(results, 'ep', split_axis=0, concat_axis=0, tiled=True)  21.7 us
    add x13, other arithmetic, link(): return (earlier[0] * later[0], later[0] * earlier[1] + later[1])  14.6 us
    unnamed x72, local copies, waits for them, and re-layouts  8.73 us
  transfers between devices with their start and end apart: 6, of which 4 were waited for; matrix products, arithmetic and copies ran while one was open for 32% of the time, Pallas kernels for 0%

profile of v1, /device:TPU:0, one launch (start us, length us, event | category | flops | bytes accessed | tf_op | source)
XLA Modules:
  0.0 311.3 jit_solution(8611729778208925656)
XLA Ops:
  11.2 2.4 scatter_custom_fusion
  15.6 6.0 %gather_fusion = bf16[1024,2048]{1,0:T(8,128)(2,1)} fusion(bf16[257,2048]{1,0:T(8,128)(2,1)S(1)} %concatenate.69, s32[1024]{0:T(1024)S(1)} %fusion.50), kind=kCustom, calls=%fused_computation | custom fusion | bytes 8392704 | tf_op jit(solution)/shard_map/gather | solution.py:111
  23.0 32.8 %all_to_all.10 = bf16[8,128,512]{2,1,0:T(8,128)(2,1)S(1)} all-to-all(bf16[8,128,512]{2,1,0:T(8,128)(2,1)S(1)} %constant_dynamic-slice_fusion.3), channel_id=1, replica_groups=mesh['ep'=8,'tp'=4] {'ep'}, dimensions={0} | all-to-all | bytes 2097152 | tf_op jit(solution)/shard_map/all_to_all | solution.py:116
  57.3 23.9 %collective-permute-done.1 = bf16[8,128,512]{2,1,0:T(8,128)(2,1)S(1)} collective-permute-done((bf16[8,128,512]{2,1,0:T(8,128)(2,1)S(1)}, bf16[8,128,512]{2,1,0:T(8,128)(2,1)S(1)}, u32[]{:S(2)}, u32[]{:S(2)}) %collective-permute-start.1) | collective-permute-done | bytes 1048608 | tf_op jit(solution)/shard_map/ppermute | solution.py:119
  83.2 23.7 %collective-permute-done.2 = bf16[8,128,512]{2,1,0:T(8,128)(2,1)} collective-permute-done((bf16[8,128,512]{2,1,0:T(8,128)(2,1)S(1)}, bf16[8,128,512]{2,1,0:T(8,128)(2,1)}, u32[]{:S(2)}, u32[]{:S(2)}) %collective-permute-start.2) | collective-permute-done | bytes 1048608 | tf_op jit(solution)/shard_map/ppermute | solution.py:119
  111.4 1.7 add_convert_fusion
  113.1 17.9 %collective-permute-done.3 = bf16[8,128,512]{2,1,0:T(8,128)(2,1)} collective-permute-done((bf16[8,128,512]{2,1,0:T(8,128)(2,1)}, bf16[8,128,512]{2,1,0:T(8,128)(2,1)}, u32[]{:S(2)}, u32[]{:S(2)}) %collective-permute-start.3) | collective-permute-done | bytes 1048608 | tf_op jit(solution)/shard_map/ppermute | solution.py:119
  137.5 2.3 fusion.10
  139.8 3.6 %multiply_convert_fusion = bf16[1024,512]{1,0:T(8,128)(2,1)} fusion(f32[1024,512]{1,0:T(8,128)S(1)} %fusion.10, bf16[1024,2048]{1,0:T(8,128)(2,1)S(1)} %bitcast.73, bf16[1,2048,512]{2,1,0:T(8,128)(2,1)S(1)} %copy-done.26), kind=kOutput, calls=%fused_computation.22 | convolution fusion | flops 2150629376 | bytes 9437184 | tf_op jit(solution)/shard_map/dot_general | solution.py:127
  146.2 1.8 convert_multiply_fusion.4
  153.4 2.0 multiply_add_fusion.1
  155.5 1.6 slice.283
  157.1 1.6 slice.284
  160.1 1.8 multiply_add_fusion.2
  163.1 1.5 slice.288
  164.6 1.5 slice.292
  166.2 1.6 multiply_add_fusion.3
  206.3 1.5 slice.287
  210.5 1.6 slice.330
  227.4 1.6 pad.114
  229.3 1.9 fusion.39
  232.0 12.8 %all-gather.1 = f32[8,1,512]{2,1,0:T(1,128)S(1)} all-gather(f32[1,1,512]{2,1,0:T(1,128)S(1)} %add_bitcast_fusion), channel_id=1, replica_groups=mesh['ep'=8,'tp'=4] {'ep'}, dimensions={0}, use_global_device_ids=true | all-gather | bytes 18432 | tf_op jit(solution)/shard_map/all_gather | solution.py:18
  244.8 1.7 pad.130
  246.5 1.6 pad.129
  248.9 12.8 %all-gather = f32[8,1,512]{2,1,0:T(1,128)S(1)} all-gather(f32[1,1,512]{2,1,0:T(1,128)S(1)} %add_bitcast_fusion.1), channel_id=1, replica_groups=mesh['ep'=8,'tp'=4] {'ep'}, dimensions={0}, use_global_device_ids=true | all-gather | bytes 18432 | tf_op jit(solution)/shard_map/all_gather | solution.py:18
  261.6 6.2 %fusion.14 = bf16[1024,512]{1,0:T(8,128)(2,1)} fusion(bf16[1024,2048]{1,0:T(8,128)(2,1)} %all-gather.4.cloned.1.call-done, bf16[1,2048,512]{2,1,0:T(8,128)(2,1)} %param.33), kind=kOutput, calls=%fused_computation.23 | convolution fusion | flops 2148007936 | bytes 7340032 | tf_op jit(solution)/shard_map/dot_general | solution.py:130
  267.9 3.9 %all-to-all-start.1 = ((bf16[8,128,512]{2,1,0:T(8,128)(2,1)}), bf16[8,128,512]{2,1,0:T(8,128)(2,1)S(1)}, u32[]{:S(2)}, u32[]{:S(2)}) async-start(bf16[8,128,512]{2,1,0:T(8,128)(2,1)} %bitcast.74), calls=%async_computation.1 | async-start | bytes 2097152 | tf_op jit(solution)/shard_map/all_to_all | solution.py:136
  272.3 4.1 %fusion.32 = bf16[256,512]{1,0:T(8,128)(2,1)} fusion(bf16[2048,512]{1,0:T(8,128)(2,1)} %param.21, f32[256,512]{1,0:T(8,128)} %pad.129, f32[256,512]{1,0:T(8,128)} %pad.130, f32[256,512]{1,0:T(8,128)} %copy-done.6, f32[256,512]{1,0:T(8,128)} %pad.114, bf16[256,2048]{1,0:T(8,128)(2,1)} %param.18, f32[2048]{0:T(1024)S(1)} %copy-done.30, ...), kind=kOutput, calls=%fused_computation.45 | convolution fusion | flops 541065216 | bytes 5516288 | tf_op jit(solution)/shard_map/dot_general | solution.py:68
  276.4 21.7 %all-to-all-done.1 = bf16[8,128,512]{2,1,0:T(8,128)(2,1)S(1)} async-done(((bf16[8,128,512]{2,1,0:T(8,128)(2,1)}), bf16[8,128,512]{2,1,0:T(8,128)(2,1)S(1)}, u32[]{:S(2)}, u32[]{:S(2)}) %all-to-all-start.1) | async-done | bytes 1048608 | tf_op jit(solution)/shard_map/all_to_all | solution.py:136
  298.1 2.6 gather_fusion.1
  300.7 1.7 reshape.120
  302.4 2.1 multiply_reduce_fusion
  (245 shorter events, 90.9 us)
Async XLA Ops:
  7.2 130.3 %copy-start = (bf16[1,2048,512]{2,1,0:T(8,128)(2,1)S(1)}, bf16[1,2048,512]{2,1,0:T(8,128)(2,1)}, u32[]{:S(2)}) copy-start(bf16[1,2048,512]{2,1,0:T(8,128)(2,1)} %param.31) | copy-start | bytes 6291460
  7.2 8.0 %copy-start.1 = (bf16[256,2048]{1,0:T(8,128)(2,1)S(1)}, bf16[256,2048]{1,0:T(8,128)(2,1)}, u32[]{:S(2)}) copy-start(bf16[256,2048]{1,0:T(8,128)(2,1)} %param.27) | copy-start | bytes 3145732
  7.2 8.0 %copy-start.14 = (f32[2048]{0:T(1024)S(1)}, f32[2048]{0:T(1024)}, u32[]{:S(2)}) copy-start(f32[2048]{0:T(1024)} %param.28) | copy-start | bytes 24580
  7.2 254.4 %all-gather.4.cloned.1.call-start = ((), (), s32[]{:S(2)}) async-start(), calls=%async_computation.2 | async-start | bytes 5242880 | tf_op jit(solution)/shard_map/all_gather | solution.py:131
  21.5 61.3 %copy-start.4 = (bf16[256,2048]{1,0:T(8,128)(2,1)S(1)}, bf16[256,2048]{1,0:T(8,128)(2,1)}, u32[]{:S(2)}) copy-start(bf16[256,2048]{1,0:T(8,128)(2,1)} %param.18) | copy-start | bytes 3145732
  23.0 84.0 %copy-start.25 = (bf16[2048,512]{1,0:T(8,128)(2,1)S(1)}, bf16[2048,512]{1,0:T(8,128)(2,1)}, u32[]{:S(2)}) copy-start(bf16[2048,512]{1,0:T(8,128)(2,1)} %param.20) | copy-start | bytes 6291460
  23.0 84.0 %copy-start.29 = (f32[2048]{0:T(1024)S(1)}, f32[2048]{0:T(1024)}, u32[]{:S(2)}) copy-start(f32[2048]{0:T(1024)} %param.19) | copy-start | bytes 24580
  55.8 25.4 %collective-permute-start.1 = (bf16[8,128,512]{2,1,0:T(8,128)(2,1)S(1)}, bf16[8,128,512]{2,1,0:T(8,128)(2,1)S(1)}, u32[]{:S(2)}, u32[]{:S(2)}) collective-permute-start(bf16[8,128,512]{2,1,0:T(8,128)(2,1)S(1)} %all_to_all.10), channel_id=1, source_target_pairs={{0,1},{1,2},{2,3},{3,0},{4,5},{5,6},{6,7},{7,4},{8,9},{9,10},{10,1... | collective-permute-start | bytes 3145736 | tf_op jit(solution)/shard_map/ppermute | solution.py:119
  82.2 24.7 %collective-permute-start.2 = (bf16[8,128,512]{2,1,0:T(8,128)(2,1)S(1)}, bf16[8,128,512]{2,1,0:T(8,128)(2,1)}, u32[]{:S(2)}, u32[]{:S(2)}) collective-permute-start(bf16[8,128,512]{2,1,0:T(8,128)(2,1)S(1)} %collective-permute-done.1), channel_id=1, source_target_pairs={{0,1},{1,2},{2,3},{3,0},{4,5},{5,6},{6,7},{7,4},{8,9},{9,10},{10,1... | collective-permute-start | bytes 3145736 | tf_op jit(solution)/shard_map/ppermute | solution.py:119
  83.1 23.8 %copy-start.23 = (f32[256]{0:T(256)}, f32[256]{0:T(256)S(1)}, u32[]{:S(2)}) copy-start(f32[256]{0:T(256)S(1)} %add_rsqrt_fusion.1) | copy-start | bytes 3076
  83.1 26.7 %copy-start.20 = (f32[256,2]{0,1:T(2,128)S(1)}, f32[256,2]{0,1:T(2,128)}, u32[]{:S(2)}) copy-start(f32[256,2]{0,1:T(2,128)} %param.30) | copy-start | bytes 6148
  83.1 26.8 %copy-start.22 = (f32[512]{0:T(512)S(1)}, f32[512]{0:T(512)}, u32[]{:S(2)}) copy-start(f32[512]{0:T(512)} %param.25) | copy-start | bytes 6148
  83.2 26.8 %copy-start.21 = (f32[4,512]{1,0:T(4,128)S(1)}, f32[4,512]{1,0:T(4,128)}, u32[]{:S(2)}) copy-start(f32[4,512]{1,0:T(4,128)} %param.22) | copy-start | bytes 24580
  106.9 24.0 %collective-permute-start.3 = (bf16[8,128,512]{2,1,0:T(8,128)(2,1)}, bf16[8,128,512]{2,1,0:T(8,128)(2,1)}, u32[]{:S(2)}, u32[]{:S(2)}) collective-permute-start(bf16[8,128,512]{2,1,0:T(8,128)(2,1)} %collective-permute-done.2), channel_id=1, source_target_pairs={{0,1},{1,2},{2,3},{3,0},{4,5},{5,6},{6,7},{7,4},{8,9},{9,10},{10,1... | collective-permute-start | bytes 3145736 | tf_op jit(solution)/shard_map/ppermute | solution.py:119
  108.4 3.0 collective-permute-start
  113.1 20.6 %copy-start.3 = (bf16[8,128,512]{2,1,0:T(8,128)(2,1)S(1)}, bf16[8,128,512]{2,1,0:T(8,128)(2,1)}, u32[]{:S(2)}) copy-start(bf16[8,128,512]{2,1,0:T(8,128)(2,1)} %copy-done.2) | copy-start | bytes 3145732
  137.5 2.3 copy-start.26
  139.8 3.6 %copy-start.27 = (bf16[4,128,128]{2,1,0:T(8,128)(2,1)S(1)}, bf16[4,128,128]{2,1,0:T(8,128)(2,1)}, u32[]{:S(2)}) copy-start(bf16[4,128,128]{2,1,0:T(8,128)(2,1)} %param.23) | copy-start | bytes 393220
  214.0 12.3 %copy-start.10 = (f32[31,512]{1,0:T(8,128)S(1)}, f32[31,512]{1,0:T(8,128)}, u32[]{:S(2)}) copy-start(f32[31,512]{1,0:T(8,128)} %slice.287) | copy-start | bytes 190468
  214.0 12.3 %copy-start.11 = (f32[31,512]{1,0:T(8,128)S(1)}, f32[31,512]{1,0:T(8,128)}, u32[]{:S(2)}) copy-start(f32[31,512]{1,0:T(8,128)} %slice.328) | copy-start | bytes 190468
  217.4 8.9 %copy-start.19 = (f32[1,512]{1,0:T(1,128)S(1)}, f32[1,512]{1,0:T(1,128)}, u32[]{:S(2)}) copy-start(f32[1,512]{1,0:T(1,128)} %slice.389) | copy-start | bytes 6148
  221.8 5.4 %copy-start.8 = (f32[63,512]{1,0:T(8,128)S(1)}, f32[63,512]{1,0:T(8,128)}, u32[]{:S(2)}) copy-start(f32[63,512]{1,0:T(8,128)} %slice.330) | copy-start | bytes 387076
  229.1 2.1 copy-start.16
  229.2 17.2 %copy-start.15 = (f32[1,512]{1,0:T(1,128)S(1)}, f32[1,512]{1,0:T(1,128)}, u32[]{:S(2)}) copy-start(f32[1,512]{1,0:T(1,128)} %slice.387) | copy-start | bytes 6148
  231.1 15.3 %copy-start.5 = (f32[127,512]{1,0:T(8,128)S(1)}, f32[127,512]{1,0:T(8,128)}, u32[]{:S(2)}) copy-start(f32[127,512]{1,0:T(8,128)} %get-tuple-element.130) | copy-start | bytes 780292
  231.3 36.6 %copy-start.6 = (f32[256,512]{1,0:T(8,128)}, f32[256,512]{1,0:T(8,128)S(1)}, u32[]{:S(2)}) copy-start(f32[256,512]{1,0:T(8,128)S(1)} %pad.113) | copy-start | bytes 1572868
  267.9 3.9 %copy-start.12 = (f32[512]{0:T(512)S(1)}, f32[512]{0:T(512)}, u32[]{:S(2)}) copy-start(f32[512]{0:T(512)} %custom-call) | copy-start | bytes 6148
  267.9 4.4 %copy-start.24 = (f32[256]{0:T(256)S(1)}, f32[256]{0:T(256)}, u32[]{:S(2)}) copy-start(f32[256]{0:T(256)} %copy-done.23) | copy-start | bytes 3076
  267.9 4.4 %copy-start.30 = (f32[2048]{0:T(1024)S(1)}, f32[2048]{0:T(1024)}, u32[]{:S(2)}) copy-start(f32[2048]{0:T(1024)} %param.19) | copy-start | bytes 24580
  267.9 30.2 %all-to-all-start.1 = ((bf16[8,128,512]{2,1,0:T(8,128)(2,1)}), bf16[8,128,512]{2,1,0:T(8,128)(2,1)S(1)}, u32[]{:S(2)}, u32[]{:S(2)}) async-start(bf16[8,128,512]{2,1,0:T(8,128)(2,1)} %bitcast.74), calls=%async_computation.1 | async-start | bytes 2097152 | tf_op jit(solution)/shard_map/all_to_all | solution.py:136
  272.3 25.8 %copy-start.13 = (s32[1024]{0:T(1024)S(1)}, s32[1024]{0:T(1024)}, u32[]{:S(2)}) copy-start(s32[1024]{0:T(1024)} %pad_clamp_fusion) | copy-start | bytes 12292
  298.1 4.3 %copy-start.7 = (f32[256,2]{1,0:T(8,128)S(1)}, f32[256,2]{1,0:T(8,128)}, u32[]{:S(2)}) copy-start(f32[256,2]{1,0:T(8,128)} %copy.41) | copy-start | bytes 6148
  (5 other events, 6.8 us)
Sparse Core Ops, SparseCore 0:
  143.6 52.2 all-gather.3
